TPU v7x, 32 devices: a whole 2x2x4 slice. The times are simulated.
32 devices in a mesh: grp: 2 (over y), sp: 4 (over z), tp: 4 (over x, core).
Axes of the slice: x: 2, y: 2, z: 4, core: 2. Of those that a mesh axis runs over, the one named last changes fastest.
Arguments:
- recurrent_query: bfloat16 [2048, 1024], P(('grp', 'sp'), 'tp'), parts along dimension 0, may hold values from -6 to 6
- recurrent_forget_gate: bfloat16 [2048, 1024], P(('grp', 'sp'), 'tp'), parts along dimension 0, may hold values from -4.5 to 4.5
- recurrent_value: bfloat16 [2048, 1024], P(('grp', 'sp'), 'tp'), parts along dimension 0, may hold values from -6 to 6
- recurrent_gate_lower_bound: float32 [1024], P('tp'), may hold values from 1.5 to 14
- recurrent_added_decay: float32 [2048, 8], P(('grp', 'sp'), 'tp'), parts along dimension 0, may hold values from -0.51 to 0
- recurrent_norm_gain: float32 [128], replicated, may hold values from 0.1 to 1.9
- attention_query_first: bfloat16 [2048, 512], P(('grp', 'sp'), 'tp'), parts along dimension 0, may hold values from -20 to 20
- attention_key_first: bfloat16 [2048, 256], P(('grp', 'sp'), 'tp'), parts along dimension 0, may hold values from -20 to 20
- attention_query_second: bfloat16 [2048, 512], P(('grp', 'sp'), 'tp'), parts along dimension 0, may hold values from -20 to 20
- attention_key_second: bfloat16 [2048, 256], P(('grp', 'sp'), 'tp'), parts along dimension 0, may hold values from -20 to 20
- attention_value: bfloat16 [2048, 512], P(('grp', 'sp'), 'tp'), parts along dimension 0, may hold values from -6 to 6
- second_map_weight: float32 [8], P('tp'), may hold values from 0.3 to 0.8
- attention_norm_gain: float32 [128], replicated, may hold values from 0.1 to 1.9
- output_weight: bfloat16 [2, 1024, 2048], P(None, 'tp', 'sp'), may hold values from -0.125 to 0.125
Outputs:
- mixed: bfloat16 [2048, 2048], P(('grp', 'sp', 'tp')), parts along dimension 0
There are 2 independent parts, one for each index of `grp`. A program takes and returns all parts, laid end to end along the dimension named above; an argument that names none is the same for every part. Nothing has to cross between parts.
All inputs are finite; a program needn't handle non-finite values.
Results may differ from a plain program's by a relative error of at most 0.02.
Values may be sent and summed in bfloat16 or wider, within the bound.
A program may use at most 64 MiB of HBM per device.

v0:
```python
import jax
import jax.numpy as jnp
from jax import lax
from jax.sharding import PartitionSpec as P

HG_DK = 128
HG_DV = 128
DA_HD = 64
BLK = 32
epsilon = 1e-06
highest = lax.Precision.HIGHEST
key_span = 512


def carried_in(array, axis, combine, identity):
    size, place = (lax.axis_size(axis), lax.axis_index(axis))
    everything = jax.tree.map(
        lambda part, kind: lax.all_gather(part.astype(kind), axis),
        array,
        (jnp.bfloat16, jnp.bfloat16),
    )
    start = jax.tree.map(
        lambda part, zero: jnp.broadcast_to(jnp.asarray(zero, part.dtype), part.shape),
        array,
        identity,
    )

    def hop(k, before):
        reached = k < place
        new = combine(
            before, jax.tree.map(lambda part, own: part[k].astype(own.dtype), everything, array)
        )
        return jax.tree.map(lambda a, b: jnp.where(reached, a, b), new, before)

    return lax.fori_loop(0, size, hop, start)


def head_norm(head_values, gain_vec):
    mean_square = jnp.mean(head_values * head_values, axis=-1, keepdims=True)
    return head_values * lax.rsqrt(mean_square + epsilon) * gain_vec


def decay_factors(gate_preactivation, lower_bound_logit, added_log_decay, number_of_heads):
    token_count = gate_preactivation.shape[0]
    floor_rate = jax.nn.sigmoid(-lower_bound_logit).reshape(number_of_heads, -1)
    state_inflow = floor_rate[None] * jax.nn.sigmoid(
        -gate_preactivation.astype(jnp.float32)
    ).reshape(token_count, number_of_heads, -1)
    decay_logarithm = jnp.log1p(-state_inflow) + added_log_decay[:, :, None]
    return (state_inflow, decay_logarithm)


def recurrence_blocks(queries, decay_logarithm, state_inflow, value_rows, block_len):
    token_count, number_of_heads, key_width = queries.shape
    block_count = token_count // block_len

    def to_blocks(source):
        return source.reshape(block_count, block_len, number_of_heads, source.shape[-1])

    causal = jnp.tril(jnp.ones((block_len, block_len), jnp.float32))[:, :, None, None]

    def block_step(carry_state, inputs):
        query_blk, decay_blk, inflow_blk, value_blk = inputs
        cumulative = jnp.cumsum(decay_blk, axis=0)
        relative = cumulative[:, None] - cumulative[None, :]
        decay_table = jnp.exp(jnp.minimum(relative, 0.0)) * causal
        scores = jnp.einsum(
            "thd,shd,tshd->hts", query_blk, inflow_blk, decay_table, precision=highest
        )
        block_out = jnp.einsum("hts,shv->thv", scores, value_blk, precision=highest)
        block_out = block_out + jnp.einsum(
            "thd,hdv->thv", query_blk * jnp.exp(cumulative), carry_state, precision=highest
        )
        last_log = cumulative[-1]
        new_state = jnp.exp(last_log)[:, :, None] * carry_state + jnp.einsum(
            "shd,shv->hdv",
            inflow_blk * jnp.exp(last_log[None] - cumulative),
            value_blk,
            precision=highest,
        )
        return (new_state, block_out)

    zero_state = jnp.zeros((number_of_heads, key_width, value_rows.shape[-1]), jnp.float32)
    final_state, outputs = lax.scan(
        block_step,
        zero_state,
        (
            to_blocks(queries),
            to_blocks(decay_logarithm),
            to_blocks(state_inflow),
            to_blocks(value_rows),
        ),
    )
    return (final_state, outputs.reshape(token_count, number_of_heads, -1))


def chain_pair(earlier, following):
    return (earlier[0] * following[0], following[0][:, :, None] * earlier[1] + following[1])


def recurrent_path_output(
    recurrent_query,
    recurrent_forget_gate,
    recurrent_value,
    recurrent_gate_lower_bound,
    recurrent_added_decay,
    recurrent_norm_gain,
):
    token_count = recurrent_query.shape[0]
    number_of_heads = recurrent_gate_lower_bound.shape[0] // HG_DK
    state_inflow, decay_logarithm = decay_factors(
        recurrent_forget_gate, recurrent_gate_lower_bound, recurrent_added_decay, number_of_heads
    )
    queries = recurrent_query.astype(jnp.float32).reshape(token_count, number_of_heads, HG_DK)
    value_rows = recurrent_value.astype(jnp.float32).reshape(token_count, number_of_heads, HG_DV)
    final_state, local_out = recurrence_blocks(
        queries, decay_logarithm, state_inflow, value_rows, BLK
    )
    running_log = jnp.cumsum(decay_logarithm, axis=0)
    through = jnp.exp(running_log[-1])
    incoming = carried_in(
        (through, final_state),
        "sp",
        chain_pair,
        (jnp.ones_like(through), jnp.zeros_like(final_state)),
    )
    carried = jnp.einsum(
        "thd,hdv->thv", queries * jnp.exp(running_log), incoming[1], precision=highest
    )
    return (
        head_norm(local_out + carried, recurrent_norm_gain)
        .astype(jnp.bfloat16)
        .reshape(token_count, -1)
    )


def attention_branch(
    attention_query_first,
    attention_key_first,
    attention_query_second,
    attention_key_second,
    attention_value,
    second_map_weight,
    attention_norm_gain,
):
    query_rows = attention_query_first.shape[0]
    key_heads = attention_key_first.shape[1] // DA_HD
    group_size = attention_query_first.shape[1] // DA_HD // key_heads
    score_scale = DA_HD ** (-0.5)
    offset = lax.axis_index("sp") * query_rows
    query_pos = offset + jnp.arange(query_rows)
    last_query = offset + query_rows - 1
    queries_one = attention_query_first.reshape(query_rows, key_heads, group_size, DA_HD)
    queries_two = attention_query_second.reshape(query_rows, key_heads, group_size, DA_HD)

    def map_update(running, queries, key_rows, value_rows, allowed):
        row_max, weight_mass, value_sum = running
        scores = (
            jnp.einsum("qkgd,skd->kgqs", queries, key_rows, preferred_element_type=jnp.float32)
            * score_scale
        )
        scores = jnp.where(allowed, scores, -1e30)
        new_max = jnp.maximum(row_max, jnp.max(scores, axis=-1))
        weights = jnp.where(allowed, jnp.exp(scores - new_max[..., None]), 0.0)
        shrink = jnp.exp(row_max - new_max)
        weight_mass = weight_mass * shrink + jnp.sum(weights, axis=-1)
        value_sum = value_sum * shrink[..., None] + jnp.einsum(
            "plew,wpd->pled",
            weights.astype(jnp.bfloat16),
            value_rows,
            preferred_element_type=jnp.float32,
        )
        return (new_max, weight_mass, value_sum)

    def key_block(running, block_one, block_two, block_values, first_row):
        span_rows = block_one.shape[0]
        key_pos = first_row + jnp.arange(span_rows)
        allowed = key_pos[None, :] <= query_pos[:, None]
        shaped_one = block_one.reshape(span_rows, key_heads, DA_HD)
        shaped_two = block_two.reshape(span_rows, key_heads, DA_HD)
        shaped_values = block_values.reshape(span_rows, key_heads, 2 * DA_HD)
        return (
            map_update(running[0], queries_one, shaped_one, shaped_values, allowed),
            map_update(running[1], queries_two, shaped_two, shaped_values, allowed),
        )

    def guarded_block(running, block_one, block_two, block_values, first_row):

        def compute(state_in):
            return key_block(state_in, block_one, block_two, block_values, first_row)

        def unchanged(state_in):
            return state_in

        result = lax.cond(first_row > last_query, unchanged, compute, running)
        return result

    start_max = jnp.full((key_heads, group_size, query_rows), -1e30, jnp.float32)
    zero_mass = jnp.zeros((key_heads, group_size, query_rows), jnp.float32)
    zero_sum = jnp.zeros((key_heads, group_size, query_rows, 2 * DA_HD), jnp.float32)
    fresh_state = (start_max, zero_mass, zero_sum)
    running = (fresh_state, fresh_state)
    shard_one = lax.all_gather(attention_key_first, "sp", axis=0, tiled=True)
    shard_two = lax.all_gather(attention_key_second, "sp", axis=0, tiled=True)
    shard_values = lax.all_gather(attention_value, "sp", axis=0, tiled=True)
    row_count = shard_one.shape[0]
    span_rows = min(row_count, key_span)
    full_count = row_count // span_rows

    def span_step(span_index, state_in):
        begin_row = span_index * span_rows
        return guarded_block(
            state_in,
            lax.dynamic_slice_in_dim(shard_one, begin_row, span_rows, 0),
            lax.dynamic_slice_in_dim(shard_two, begin_row, span_rows, 0),
            lax.dynamic_slice_in_dim(shard_values, begin_row, span_rows, 0),
            begin_row,
        )

    running = lax.fori_loop(0, full_count, span_step, running)
    first_map, second_map = running
    lambda_table = second_map_weight.reshape(key_heads, group_size)[:, :, None, None]
    combined = first_map[2] / first_map[1][..., None] - lambda_table * (
        second_map[2] / second_map[1][..., None]
    )
    combined = jnp.transpose(combined, (2, 0, 1, 3)).reshape(
        query_rows, key_heads * group_size, 2 * DA_HD
    )
    return head_norm(combined, attention_norm_gain).astype(jnp.bfloat16).reshape(query_rows, -1)


def shards(
    recurrent_query,
    recurrent_forget_gate,
    recurrent_value,
    recurrent_gate_lower_bound,
    recurrent_added_decay,
    recurrent_norm_gain,
    attention_query_first,
    attention_key_first,
    attention_query_second,
    attention_key_second,
    attention_value,
    second_map_weight,
    attention_norm_gain,
    output_weight,
):
    attended = attention_branch(
        attention_query_first,
        attention_key_first,
        attention_query_second,
        attention_key_second,
        attention_value,
        second_map_weight,
        attention_norm_gain,
    )
    recurrent_output = recurrent_path_output(
        recurrent_query,
        recurrent_forget_gate,
        recurrent_value,
        recurrent_gate_lower_bound,
        recurrent_added_decay,
        recurrent_norm_gain,
    )
    pieces = lax.all_gather(output_weight, "sp", axis=2, tiled=True)
    partial_terms = jnp.dot(
        recurrent_output, pieces[0], preferred_element_type=jnp.float32
    ) + jnp.dot(attended, pieces[1], preferred_element_type=jnp.float32)
    return lax.psum_scatter(
        partial_terms.astype(jnp.bfloat16), "tp", scatter_dimension=0, tiled=True
    )


def solution(mesh):
    return jax.shard_map(
        shards,
        mesh=mesh,
        in_specs=(
            P(("grp", "sp"), "tp"),
            P(("grp", "sp"), "tp"),
            P(("grp", "sp"), "tp"),
            P("tp"),
            P(("grp", "sp"), "tp"),
            P(),
            P(("grp", "sp"), "tp"),
            P(("grp", "sp"), "tp"),
            P(("grp", "sp"), "tp"),
            P(("grp", "sp"), "tp"),
            P(("grp", "sp"), "tp"),
            P("tp"),
            P(),
            P(None, "tp", "sp"),
        ),
        out_specs=P(("grp", "sp", "tp"), None),
        check_vma=False,
    )
```

profile of v0, /device:TPU:0, one launch (start us, length us, event | category | flops | bytes accessed | tf_op | source)
XLA Modules:
  0.0 149.0 jit_solution(5763729873363414824)
XLA Ops:
  6.5 0.7 all-gather.3.cloned.1.call-update
  7.3 0.7 divide_bitcast_fusion
  8.0 1.0 copy.151
  9.0 1.0 copy.148
  10.1 15.8 %all_gather.26 = bf16[1024,64]{0,1:T(8,128)(2,1)S(1)} all-gather(bf16[256,64]{0,1:T(8,128)(2,1)} %param.29), channel_id=1, replica_groups=mesh['grp'=2,'sp'=4,'tp'=4] {'sp'}, dimensions={0}, use_global_device_ids=true | all-gather | bytes 163840 | tf_op jit(solution)/shard_map/all_gather | solution.py:203
  25.9 0.8 copy.178
  28.4 16.7 %all_gather.27 = bf16[1024,128]{1,0:T(8,128)(2,1)S(1)} all-gather(bf16[256,128]{1,0:T(8,128)(2,1)S(1)} %copy-done.2), channel_id=1, replica_groups=mesh['grp'=2,'sp'=4,'tp'=4] {'sp'}, dimensions={0}, use_global_device_ids=true | all-gather | bytes 327680 | tf_op jit(solution)/shard_map/all_gather | solution.py:205
  45.1 0.5 log-plus-one_add_fusion
  45.6 24.4 %while.52 = (s32[]{:T(128)}, f32[2,128,128]{2,1,0:T(8,128)S(1)}, f32[8,32,2,128]{3,1,0,2:T(8,128)S(1)}, f32[8,32,2,128]{3,2,1,0:T(2,128)S(1)}, f32[8,32,2,128]{3...) while((s32[]{:T(128)}, f32[2,128,128]{2,1,0:T(8,128)S(1)}, ...), condition=%wide.region_2.3_spmd.clone, body=%wide.region_0.2_spmd.clone.sunk | while | flops 30302212 | bytes 3405956 | solution.py:84
  45.8 1.2 multiply_bitcast_fusion.2
  47.0 0.7 fusion.91
  48.2 0.4 convolution_add_fusion.3
  48.8 1.2 multiply_bitcast_fusion.2
  50.1 0.7 fusion.91
  51.3 0.4 convolution_add_fusion.3
  51.9 1.2 multiply_bitcast_fusion.2
  53.1 0.7 fusion.91
  54.3 0.4 convolution_add_fusion.3
  54.9 1.2 multiply_bitcast_fusion.2
  56.2 0.7 fusion.91
  57.4 0.4 convolution_add_fusion.3
  58.0 1.2 multiply_bitcast_fusion.2
  59.2 0.7 fusion.91
  60.4 0.4 convolution_add_fusion.3
  61.0 1.2 multiply_bitcast_fusion.2
  62.3 0.7 fusion.91
  63.5 0.4 convolution_add_fusion.3
  64.1 1.2 multiply_bitcast_fusion.2
  65.3 0.7 fusion.91
  66.5 0.4 convolution_add_fusion.3
  67.1 1.2 multiply_bitcast_fusion.2
  68.4 0.7 fusion.91
  69.6 0.4 convolution_add_fusion.3
  70.0 13.4 %all_gather.28 = bf16[1024,64]{0,1:T(8,128)(2,1)S(1)} all-gather(bf16[256,64]{0,1:T(8,128)(2,1)S(1)} %copy-done.5), channel_id=1, replica_groups=mesh['grp'=2,'sp'=4,'tp'=4] {'sp'}, dimensions={0}, use_global_device_ids=true | all-gather | bytes 163840 | tf_op jit(solution)/shard_map/all_gather | solution.py:204
  84.0 2.5 %while.51 = (s32[]{:T(128)}, f32[1,2,256]{2,1,0:T(2,128)S(1)}, f32[1,2,256]{2,1,0:T(2,128)S(1)}, f32[1,2,256,128]{3,2,1,0:T(8,128)S(1)}, f32[1,2,256]{2,1,0:T(2,...) while((s32[]{:T(128)}, f32[1,2,256]{2,1,0:T(2,128)S(1)}, ...), condition=%wide.region_15.16_spmd.clone, body=%wide.region_8.15_spmd.clone.sunk | while | flops 206442240 | bytes 8724921 | solution.py:220
  84.0 2.3 %conditional.3 = (f32[1,2,256]{2,1,0:T(2,128)S(1)}, f32[1,2,256]{2,1,0:T(2,128)S(1)}, f32[1,2,256,128]{3,2,1,0:T(8,128)S(1)}, f32[1,2,256]{2,1,0:T(2,128)S(1)}, ...) conditional(s32[]{:T(128)} %convert_element_type.97, (s32[]{:T(128)}, s32[]{:T(128)}, ...), branch_computations={%region_9.13_spmd, %region_14.14_spmd} | conditional | flops 206442240 | bytes 8715370 | solution.py:195
  84.2 0.3 fusion.69
  84.6 0.5 fusion.9
  85.1 0.3 fusion.68
  85.4 0.4 fusion.13
  85.8 0.5 fusion.8
  86.9 13.0 %all_gather.22 = bf16[4,2,128]{2,1,0:T(2,128)(2,1)S(1)} all-gather(bf16[1,2,128]{2,1,0:T(2,128)(2,1)S(1)} %fusion.67), channel_id=1, replica_groups=mesh['grp'=2,'sp'=4,'tp'=4] {'sp'}, dimensions={0}, use_global_device_ids=true | all-gather | bytes 2560 | tf_op jit(solution)/shard_map/all_gather | solution.py:18
  99.9 13.8 %all-gather = bf16[8,128,128]{2,1,0:T(8,128)(2,1)S(1)} all-gather(bf16[2,128,128]{2,1,0:T(8,128)(2,1)S(1)} %convert_element_type.73), channel_id=2, replica_groups=mesh['grp'=2,'sp'=4,'tp'=4] {'sp'}, dimensions={0}, use_global_device_ids=true | all-gather | bytes 327680 | tf_op jit(solution)/shard_map/all_gather | solution.py:18
  114.2 0.7 while.53
  114.9 0.4 multiply_reduce_fusion
  115.6 1.8 %fusion.60 = f32[256,2048]{1,0:T(8,128)S(1)} fusion(bf16[256,256]{0,1:T(8,128)(2,1)S(1)} %bitcast.210, bf16[2,256,2048]{2,1,0:T(8,128)(2,1)} %all-gather.3.cloned.1.call-done), kind=kOutput, calls=%fused_computation.91 | convolution fusion | flops 268435456 | bytes 3276800 | tf_op jit(solution)/shard_map/dot_general | solution.py:266
  117.5 1.4 fusion.58
  119.0 23.2 %reduce-scatter.2.cloned.1.call-done = bf16[64,2048]{1,0:T(8,128)(2,1)} async-done(((bf16[256,2048]{1,0:T(8,128)(2,1)}), bf16[64,2048]{1,0:T(8,128)(2,1)}) %reduce-scatter.2.cloned.1.call-update) | async-done | bytes 262160 | tf_op jit(solution)/shard_map/reduce_scatter | solution.py:269
  (174 shorter events, 8.9 us)
Async XLA Ops:
  6.5 20.3 %copy-start.6 = (f32[256,2]{0,1:T(2,128)S(1)}, f32[256,2]{0,1:T(2,128)}, u32[]{:S(2)}) copy-start(f32[256,2]{0,1:T(2,128)} %param.26) | copy-start | bytes 6148
  6.5 109.0 %all-gather.3.cloned.1.call-start = ((), (), s32[]{:S(2)}) async-start(), calls=%async_computation.1 | async-start | bytes 2621440 | tf_op jit(solution)/shard_map/all_gather | solution.py:265
  7.3 134.9 %reduce-scatter.2.cloned.1.call-start = ((), (), s32[]{:S(2)}) async-start(), calls=%async_computation.2 | async-start | bytes 1310720 | tf_op jit(solution)/shard_map/reduce_scatter | solution.py:269
  27.1 1.2 copy-start.1
  27.2 1.2 copy-start.2
  45.5 24.5 %copy-start.5 = (bf16[256,64]{0,1:T(8,128)(2,1)S(1)}, bf16[256,64]{0,1:T(8,128)(2,1)}, u32[]{:S(2)}) copy-start(bf16[256,64]{0,1:T(8,128)(2,1)} %param.31) | copy-start | bytes 98308
  45.5 37.9 %copy-start.3 = (bf16[256,128]{1,0:T(8,128)(2,1)S(1)}, bf16[256,128]{1,0:T(8,128)(2,1)}, u32[]{:S(2)}) copy-start(bf16[256,128]{1,0:T(8,128)(2,1)} %param.28) | copy-start | bytes 196612
  45.6 38.0 %copy-start.4 = (bf16[256,128]{1,0:T(8,128)(2,1)S(1)}, bf16[256,128]{1,0:T(8,128)(2,1)}, u32[]{:S(2)}) copy-start(bf16[256,128]{1,0:T(8,128)(2,1)} %param.30) | copy-start | bytes 196612
  86.5 27.2 %copy-start.9 = (f32[2]{0:T(128)S(1)}, f32[2]{0:T(128)}, u32[]{:S(2)}) copy-start(f32[2]{0:T(128)} %param.33) | copy-start | bytes 28
  113.7 1.6 %copy-start.7 = (f32[128]{0:T(128)S(1)}, f32[128]{0:T(128)}, u32[]{:S(2)}) copy-start(f32[128]{0:T(128)} %param.34) | copy-start | bytes 1540
  113.8 1.6 %copy-start.8 = (f32[128]{0:T(128)S(1)}, f32[128]{0:T(128)}, u32[]{:S(2)}) copy-start(f32[128]{0:T(128)} %param.27) | copy-start | bytes 1540
  115.6 1.9 %copy-start = (bf16[2,256,2048]{2,1,0:T(8,128)(2,1)S(1)}, bf16[2,256,2048]{2,1,0:T(8,128)(2,1)}, u32[]{:S(2)}) copy-start(bf16[2,256,2048]{2,1,0:T(8,128)(2,1)} %all-gather.3.cloned.1.call-done) | copy-start | bytes 6291460
Sparse Core Ops, SparseCore 0:
  8.9 53.0 all-gather.2
  119.1 23.0 reduce-scatter.1
where the time goes:
time: 149 us
  blocking collectives  72.7 us (49%)
  waiting for transfers between devices  24 us (16%)
  other arithmetic  19.9 us (13%)
  between operations  13.9 us (9%)
  matrix products  12.3 us (8%)
  local copies, waits for them, and re-layouts  5.09 us (3%)
    all_gather x2, blocking collectives, carried_in(): lax.all_gather(part.astype(kind), axis)  26.8 us
    reduce_scatter x1, waiting for transfers between devices, shards(): lax.psum_scatter(partial_terms.astype(jnp.bfloat16), 'tp', scatter_dimens...  23.2 us
    all_gather x1, blocking collectives, attention_branch(): shard_values = lax.all_gather(attention_value, 'sp', axis=0, tiled=True)  16.7 us
    all_gather x1, blocking collectives, attention_branch(): shard_one = lax.all_gather(attention_key_first, 'sp', axis=0, tiled=True)  15.8 us
    all_gather x1, blocking collectives, attention_branch(): shard_two = lax.all_gather(attention_key_second, 'sp', axis=0, tiled=True)  13.4 us
    while x8, other arithmetic  9.95 us
    dot_general x8, other arithmetic, block_step(): jnp.einsum('thd,shd,tshd->hts', query_blk, inflow_blk, decay_table, preci...  5.65 us
    dot_general x8, matrix products, block_step(): jnp.einsum('shd,shv->hdv', inflow_blk * jnp.exp(last_log[None] - cumulati...  3.16 us
  transfers between devices with their start and end apart: 2, of which 1 were waited for; matrix products, arithmetic and copies ran while one was open for 23% of the time, Pallas kernels for 0%

commit v1 on v0

--- a/solution.py
+++ b/solution.py
@@ -200,7 +200,12 @@
     zero_sum = jnp.zeros((key_heads, group_size, query_rows, 2 * DA_HD), jnp.float32)
     fresh_state = (start_max, zero_mass, zero_sum)
     running = (fresh_state, fresh_state)
-    shard_one = lax.all_gather(attention_key_first, "sp", axis=0, tiled=True)
+    ring = [attention_key_first]
+    for hop_ in range(3):
+        ring.append(lax.ppermute(ring[-1], "sp", [(dev, (dev + 1) % 4) for dev in range(4)]))
+    shard_one = jnp.roll(
+        jnp.concatenate(ring[::-1], axis=0), (lax.axis_index("sp") + 1) * ring[0].shape[0], axis=0
+    )
     shard_two = lax.all_gather(attention_key_second, "sp", axis=0, tiled=True)
     shard_values = lax.all_gather(attention_value, "sp", axis=0, tiled=True)
     row_count = shard_one.shape[0]

time: 149 us -> 137 us (0.919)
  blocking collectives: 72.7 us -> 54.9 us
  starting transfers between devices: 0.04 us -> 5.09 us
  waiting for transfers between devices: 24 us -> 26.9 us
  local copies, waits for them, and re-layouts: 5.09 us -> 3.52 us
    all_gather x1 -> x0, blocking collectives: 15.8 us -> none  [attention_branch(): shard_one = lax.all_gather(attention_key_first, 'sp', axis=0, tiled=True)]
    ppermute x0 -> x3, starting transfers between devices: none -> 5.01 us  [attention_branch(): lax.ppermute(ring[-1], 'sp', [(dev, (dev + 1) % 4) for dev in range(4)])]
    reduce_scatter x1, waiting for transfers between devices: 23.2 us -> 26.8 us  [shards(): lax.psum_scatter(partial_terms.astype(jnp.bfloat16), 'tp', scatter_dimens...]
    all_gather x1, blocking collectives: 16.7 us -> 14.5 us  [attention_branch(): shard_values = lax.all_gather(attention_value, 'sp', axis=0, tiled=True)]
  transfers between devices with their start and end apart: 2 -> 5, of which waited for: 1 -> 1; matrix products, arithmetic and copies ran while one was open for 23% -> 23% of each run, Pallas kernels for 0% -> 0%
where the time goes in v1:
time: 137 us
  blocking collectives  54.9 us (40%)
  waiting for transfers between devices  26.9 us (20%)
  other arithmetic  19.2 us (14%)
  between operations  14 us (10%)
  matrix products  12.3 us (9%)
  starting transfers between devices  5.09 us (4%)
  local copies, waits for them, and re-layouts  3.52 us (3%)
    all_gather x2, blocking collectives, carried_in(): lax.all_gather(part.astype(kind), axis)  26.9 us
    reduce_scatter x1, waiting for transfers between devices, shards(): lax.psum_scatter(partial_terms.astype(jnp.bfloat16), 'tp', scatter_dimens...  26.8 us
    all_gather x1, blocking collectives, attention_branch(): shard_values = lax.all_gather(attention_value, 'sp', axis=0, tiled=True)  14.5 us
    all_gather x1, blocking collectives, attention_branch(): shard_two = lax.all_gather(attention_key_second, 'sp', axis=0, tiled=True)  13.5 us
    while x8, other arithmetic  9.95 us
    dot_general x8, other arithmetic, block_step(): jnp.einsum('thd,shd,tshd->hts', query_blk, inflow_blk, decay_table, preci...  5.65 us
    ppermute x3, starting transfers between devices, attention_branch(): lax.ppermute(ring[-1], 'sp', [(dev, (dev + 1) % 4) for dev in range(4)])  5.01 us
    dot_general x8, matrix products, block_step(): jnp.einsum('shd,shv->hdv', inflow_blk * jnp.exp(last_log[None] - cumulati...  3.15 us
  transfers between devices with their start and end apart: 5, of which 1 were waited for; matrix products, arithmetic and copies ran while one was open for 23% of the time, Pallas kernels for 0%

profile of v1, /device:TPU:0, one launch (start us, length us, event | category | flops | bytes accessed | tf_op | source)
XLA Modules:
  0.0 137.0 jit_solution(8199558663500702932)
XLA Ops:
  6.6 3.1 %collective-permute-start = (bf16[256,64]{0,1:T(8,128)(2,1)}, bf16[256,64]{0,1:T(8,128)(2,1)S(1)}, u32[]{:S(2)}, u32[]{:S(2)}) collective-permute-start(bf16[256,64]{0,1:T(8,128)(2,1)} %param.29), channel_id=1, source_target_pairs={{0,4},{4,8},{8,12},{12,0},{1,5},{5,9},{9,13},{13,1},{2,6},{6,10},{... | collective-permute-start | bytes 98312 | tf_op jit(solution)/shard_map/ppermute | solution.py:205
  9.8 1.0 copy.148
  11.9 0.5 log-plus-one_add_fusion
  12.3 24.4 %while.52 = (s32[]{:T(128)}, f32[2,128,128]{2,1,0:T(8,128)S(1)}, f32[8,32,2,128]{3,1,0,2:T(8,128)S(1)}, f32[8,32,2,128]{3,2,1,0:T(2,128)S(1)}, f32[8,32,2,128]{3...) while((s32[]{:T(128)}, f32[2,128,128]{2,1,0:T(8,128)S(1)}, ...), condition=%wide.region_2.3_spmd.clone, body=%wide.region_0.2_spmd.clone.sunk | while | flops 30302212 | bytes 3405948 | solution.py:84
  12.4 1.2 multiply_bitcast_fusion.2
  13.7 0.7 fusion.91
  14.4 0.2 convolution_bitcast_fusion.6
  14.7 0.2 fusion.92
  15.0 0.4 convolution_add_fusion.3
  15.5 1.2 multiply_bitcast_fusion.2
  16.7 0.7 fusion.91
  18.0 0.4 convolution_add_fusion.3
  18.5 1.2 multiply_bitcast_fusion.2
  19.8 0.7 fusion.91
  21.1 0.4 convolution_add_fusion.3
  21.6 1.2 multiply_bitcast_fusion.2
  22.8 0.7 fusion.91
  24.1 0.4 convolution_add_fusion.3
  24.6 1.2 multiply_bitcast_fusion.2
  25.9 0.7 fusion.91
  27.2 0.4 convolution_add_fusion.3
  27.7 1.2 multiply_bitcast_fusion.2
  28.9 0.7 fusion.91
  30.2 0.4 convolution_add_fusion.3
  30.7 1.2 multiply_bitcast_fusion.2
  32.0 0.7 fusion.91
  33.3 0.4 convolution_add_fusion.3
  33.8 1.2 multiply_bitcast_fusion.2
  35.0 0.7 fusion.91
  36.3 0.4 convolution_add_fusion.3
  36.7 16.3 %all-gather = bf16[8,128,128]{2,1,0:T(8,128)(2,1)S(1)} all-gather(bf16[2,128,128]{2,1,0:T(8,128)(2,1)S(1)} %convert_element_type.73), channel_id=2, replica_groups=mesh['grp'=2,'sp'=4,'tp'=4] {'sp'}, dimensions={0}, use_global_device_ids=true | all-gather | bytes 327680 | tf_op jit(solution)/shard_map/all_gather | solution.py:18
  54.0 10.6 %all_gather.19 = bf16[4,2,128]{2,1,0:T(2,128)(2,1)S(1)} all-gather(bf16[1,2,128]{2,1,0:T(2,128)(2,1)S(1)} %fusion.67), channel_id=1, replica_groups=mesh['grp'=2,'sp'=4,'tp'=4] {'sp'}, dimensions={0}, use_global_device_ids=true | all-gather | bytes 2560 | tf_op jit(solution)/shard_map/all_gather | solution.py:18
  64.6 0.7 while.53
  65.6 0.3 exponential_multiply_fusion
  65.9 0.4 multiply_reduce_fusion
  66.6 14.5 %all_gather.23 = bf16[1024,128]{1,0:T(8,128)(2,1)S(1)} all-gather(bf16[256,128]{1,0:T(8,128)(2,1)S(1)} %copy-done.4), channel_id=1, replica_groups=mesh['grp'=2,'sp'=4,'tp'=4] {'sp'}, dimensions={0}, use_global_device_ids=true | all-gather | bytes 327680 | tf_op jit(solution)/shard_map/all_gather | solution.py:210
  81.3 1.8 %collective-permute-start.2 = (bf16[256,64]{0,1:T(8,128)(2,1)S(1)}, bf16[256,64]{0,1:T(8,128)(2,1)S(1)}, u32[]{:S(2)}, u32[]{:S(2)}) collective-permute-start(bf16[256,64]{0,1:T(8,128)(2,1)S(1)} %collective-permute-done.1), channel_id=1, source_target_pairs={{0,4},{4,8},{8,12},{12,0},{1,5},{5,9},{9,13},{13,1},{2,6},{6,10},{... | collective-permute-start | bytes 98312 | tf_op jit(solution)/shard_map/ppermute | solution.py:205
  83.2 13.5 %all_gather.24 = bf16[1024,64]{0,1:T(8,128)(2,1)S(1)} all-gather(bf16[256,64]{0,1:T(8,128)(2,1)S(1)} %copy-done.7), channel_id=1, replica_groups=mesh['grp'=2,'sp'=4,'tp'=4] {'sp'}, dimensions={0}, use_global_device_ids=true | all-gather | bytes 163840 | tf_op jit(solution)/shard_map/all_gather | solution.py:209
  96.9 2.5 %while.51 = (s32[]{:T(128)}, f32[1,2,256]{2,1,0:T(2,128)S(1)}, f32[1,2,256]{2,1,0:T(2,128)S(1)}, f32[1,2,256,128]{3,2,1,0:T(8,128)S(1)}, f32[1,2,256]{2,1,0:T(2,...) while((s32[]{:T(128)}, f32[1,2,256]{2,1,0:T(2,128)S(1)}, ...), condition=%wide.region_15.16_spmd.clone, body=%wide.region_8.15_spmd.clone.sunk | while | flops 206442240 | bytes 8724921 | solution.py:225
  96.9 2.3 %conditional.3 = (f32[1,2,256]{2,1,0:T(2,128)S(1)}, f32[1,2,256]{2,1,0:T(2,128)S(1)}, f32[1,2,256,128]{3,2,1,0:T(8,128)S(1)}, f32[1,2,256]{2,1,0:T(2,128)S(1)}, ...) conditional(s32[]{:T(128)} %convert_element_type.97, (s32[]{:T(128)}, s32[]{:T(128)}, ...), branch_computations={%region_9.13_spmd, %region_14.14_spmd} | conditional | flops 206442240 | bytes 8715370 | solution.py:195
  97.1 0.3 fusion.69
  97.5 0.5 fusion.9
  98.0 0.3 fusion.68
  98.3 0.5 fusion.8
  98.8 0.4 fusion.13
  100.0 1.8 %fusion.60 = f32[256,2048]{1,0:T(8,128)S(1)} fusion(bf16[256,256]{0,1:T(8,128)(2,1)S(1)} %bitcast.209, bf16[2,256,2048]{2,1,0:T(8,128)(2,1)} %all-gather.3.cloned.1.call-done), kind=kOutput, calls=%fused_computation.91 | convolution fusion | flops 268435456 | bytes 3276800 | tf_op jit(solution)/shard_map/dot_general | solution.py:271
  101.9 1.4 %fusion.58 = bf16[256,2048]{1,0:T(8,128)(2,1)} fusion(f32[256,2048]{1,0:T(8,128)S(1)} %fusion.60, bf16[256,256]{0,1:T(8,128)(2,1)S(1)} %bitcast.210, bf16[2,256,2048]{2,1,0:T(8,128)(2,1)S(1)} %copy-done), kind=kOutput, calls=%fused_computation.86 | convolution fusion | flops 269484032 | bytes 4325376 | tf_op jit(solution)/shard_map/dot_general | solution.py:273
  103.3 26.8 %reduce-scatter.2.cloned.1.call-done = bf16[64,2048]{1,0:T(8,128)(2,1)} async-done(((bf16[256,2048]{1,0:T(8,128)(2,1)}), bf16[64,2048]{1,0:T(8,128)(2,1)}) %reduce-scatter.2.cloned.1.call-update) | async-done | bytes 262160 | tf_op jit(solution)/shard_map/reduce_scatter | solution.py:274
  (194 shorter events, 8.5 us)
Async XLA Ops:
  6.5 4.6 %copy-start.9 = (f32[256]{0:T(256)S(1)}, f32[256]{0:T(256)}, u32[]{:S(2)}) copy-start(f32[256]{0:T(256)} %param.25) | copy-start | bytes 3076
  6.5 4.7 %copy-start.8 = (f32[256,2]{0,1:T(2,128)S(1)}, f32[256,2]{0,1:T(2,128)}, u32[]{:S(2)}) copy-start(f32[256,2]{0,1:T(2,128)} %param.26) | copy-start | bytes 6148
  6.5 4.8 %copy-start.2 = (bf16[256,256]{1,0:T(8,128)(2,1)S(1)}, bf16[256,256]{1,0:T(8,128)(2,1)}, u32[]{:S(2)}) copy-start(bf16[256,256]{1,0:T(8,128)(2,1)} %param.22) | copy-start | bytes 393220
  6.5 5.2 %copy-start.1 = (bf16[256,256]{1,0:T(8,128)(2,1)S(1)}, bf16[256,256]{1,0:T(8,128)(2,1)}, u32[]{:S(2)}) copy-start(bf16[256,256]{1,0:T(8,128)(2,1)} %param.24) | copy-start | bytes 393220
  6.5 93.4 %all-gather.3.cloned.1.call-start = ((), (), s32[]{:S(2)}) async-start(), calls=%async_computation.1 | async-start | bytes 2621440 | tf_op jit(solution)/shard_map/all_gather | solution.py:270
  6.6 59.9 %collective-permute-start = (bf16[256,64]{0,1:T(8,128)(2,1)}, bf16[256,64]{0,1:T(8,128)(2,1)S(1)}, u32[]{:S(2)}, u32[]{:S(2)}) collective-permute-start(bf16[256,64]{0,1:T(8,128)(2,1)} %param.29), channel_id=1, source_target_pairs={{0,4},{4,8},{8,12},{12,0},{1,5},{5,9},{9,13},{13,1},{2,6},{6,10},{... | collective-permute-start | bytes 98312 | tf_op jit(solution)/shard_map/ppermute | solution.py:205
  9.7 120.4 %reduce-scatter.2.cloned.1.call-start = ((), (), s32[]{:S(2)}) async-start(), calls=%async_computation.2 | async-start | bytes 1310720 | tf_op jit(solution)/shard_map/reduce_scatter | solution.py:274
  64.6 1.8 %copy-start.10 = (f32[128]{0:T(128)S(1)}, f32[128]{0:T(128)}, u32[]{:S(2)}) copy-start(f32[128]{0:T(128)} %param.27) | copy-start | bytes 1540
  65.2 1.3 copy-start.4
  65.2 15.8 %copy-start.5 = (bf16[256,128]{1,0:T(8,128)(2,1)S(1)}, bf16[256,128]{1,0:T(8,128)(2,1)}, u32[]{:S(2)}) copy-start(bf16[256,128]{1,0:T(8,128)(2,1)} %param.28) | copy-start | bytes 196612
  65.3 15.9 %copy-start.6 = (bf16[256,128]{1,0:T(8,128)(2,1)S(1)}, bf16[256,128]{1,0:T(8,128)(2,1)}, u32[]{:S(2)}) copy-start(bf16[256,128]{1,0:T(8,128)(2,1)} %param.30) | copy-start | bytes 196612
  65.3 17.9 %copy-start.7 = (bf16[256,64]{0,1:T(8,128)(2,1)S(1)}, bf16[256,64]{0,1:T(8,128)(2,1)}, u32[]{:S(2)}) copy-start(bf16[256,64]{0,1:T(8,128)(2,1)} %param.31) | copy-start | bytes 98308
  65.3 31.4 %copy-start.3 = (bf16[256,64]{0,1:T(8,128)(2,1)S(1)}, bf16[256,64]{0,1:T(8,128)(2,1)}, u32[]{:S(2)}) copy-start(bf16[256,64]{0,1:T(8,128)(2,1)} %param.29) | copy-start | bytes 98308
  66.5 14.9 %collective-permute-start.1 = (bf16[256,64]{0,1:T(8,128)(2,1)S(1)}, bf16[256,64]{0,1:T(8,128)(2,1)S(1)}, u32[]{:S(2)}, u32[]{:S(2)}) collective-permute-start(bf16[256,64]{0,1:T(8,128)(2,1)S(1)} %collective-permute-done), channel_id=1, source_target_pairs={{0,4},{4,8},{8,12},{12,0},{1,5},{5,9},{9,13},{13,1},{2,6},{6,10},{... | collective-permute-start | bytes 98312 | tf_op jit(solution)/shard_map/ppermute | solution.py:205
  81.3 15.3 %collective-permute-start.2 = (bf16[256,64]{0,1:T(8,128)(2,1)S(1)}, bf16[256,64]{0,1:T(8,128)(2,1)S(1)}, u32[]{:S(2)}, u32[]{:S(2)}) collective-permute-start(bf16[256,64]{0,1:T(8,128)(2,1)S(1)} %collective-permute-done.1), channel_id=1, source_target_pairs={{0,4},{4,8},{8,12},{12,0},{1,5},{5,9},{9,13},{13,1},{2,6},{6,10},{... | collective-permute-start | bytes 98312 | tf_op jit(solution)/shard_map/ppermute | solution.py:205
  96.9 2.8 %copy-start.12 = (f32[2]{0:T(128)S(1)}, f32[2]{0:T(128)}, u32[]{:S(2)}) copy-start(f32[2]{0:T(128)} %param.33) | copy-start | bytes 28
  96.9 2.9 %copy-start.11 = (f32[128]{0:T(128)S(1)}, f32[128]{0:T(128)}, u32[]{:S(2)}) copy-start(f32[128]{0:T(128)} %param.34) | copy-start | bytes 1540
  99.9 1.9 %copy-start = (bf16[2,256,2048]{2,1,0:T(8,128)(2,1)S(1)}, bf16[2,256,2048]{2,1,0:T(8,128)(2,1)}, u32[]{:S(2)}) copy-start(bf16[2,256,2048]{2,1,0:T(8,128)(2,1)} %all-gather.3.cloned.1.call-done) | copy-start | bytes 6291460
Sparse Core Ops, SparseCore 0:
  9.8 51.6 all-gather.2
  103.4 26.6 reduce-scatter.1
